TPU v7x, 512 devices: a whole 4x4x16 slice. The times are simulated.
512 devices in a mesh: sp: 256 (over z, y, x), tp: 2 (over core).
Axes of the slice: x: 4, y: 4, z: 16, core: 2. Of those that a mesh axis runs over, the one named last changes fastest.
Arguments:
- query_rows: bfloat16 [65536, 1024], P('sp', 'tp'), may hold values from -6 to 6
- key_rows: bfloat16 [65536, 1024], P('sp', 'tp'), may hold values from -6 to 6
- value_rows: bfloat16 [65536, 1024], P('sp', 'tp'), may hold values from -6 to 6
- out_weight: bfloat16 [1024, 2048], P('tp'), may hold values from -0.75 to 0.75
Outputs:
- layer_out: bfloat16 [65536, 2048], P(('sp', 'tp'))
All inputs are finite; a program needn't handle non-finite values.
Results may differ from a plain program's by a relative error of at most 0.012.
Values may be sent and summed in bfloat16 or wider, within the bound.
No kernel may reach another device: no remote copies, remote signals or barrier semaphores. Data moves between devices by JAX's collectives and lax.ppermute only.
A program may use at most 64 MiB of HBM per device.

v0:
```python
import math
import jax
import jax.numpy as jnp
from jax import lax
from jax.sharding import PartitionSpec as P

HD = 64
BACK = 128
THETA = 500000.0
DILATIONS = (1, 4, 16)


def shifted(value, axis, steps):
    count = lax.axis_size(axis)
    initial, last = (max(0, -steps), min(count, count - steps))
    return lax.ppermute(value, axis, [(source, source + steps) for source in range(initial, last)])


def rotate(rows, positions, head_count, head_dim):
    half_dim = head_dim // 2
    inverse = jnp.power(jnp.float32(THETA), -jnp.arange(half_dim, dtype=jnp.float32) / half_dim)
    angles = positions.astype(jnp.float32)[:, None] * inverse[None, :]
    cosine = jnp.cos(angles)[:, None, :]
    sine = jnp.sin(angles)[:, None, :]
    whole = rows.astype(jnp.float32).reshape(rows.shape[0], head_count, head_dim)
    lower = whole[..., :half_dim]
    upper = whole[..., half_dim:]
    turned = jnp.concatenate(
        [lower * cosine - upper * sine, upper * cosine + lower * sine], axis=-1
    )
    return turned.reshape(rows.shape[0], head_count * head_dim).astype(jnp.bfloat16)


def pattern_part(queries, key_ext, value_ext, dilation, anchor, head_count):
    tok_rows = queries.shape[0]
    length = tok_rows // dilation
    nblocks = max(1, length // BACK)
    block_rows = length // nblocks
    query_sub = queries.reshape(length, dilation, head_count, HD)
    key_sub = key_ext.reshape(BACK + length, dilation, head_count, HD)
    value_sub = value_ext.reshape(BACK + length, dilation, head_count, HD)
    residues = jnp.arange(dilation, dtype=jnp.int32)[:, None, None, None]
    results, maxima, sums = ([], [], [])
    for block_index in range(nblocks):
        first_row = block_index * block_rows
        key_part = key_sub[first_row : first_row + BACK + block_rows]
        value_part = value_sub[first_row : first_row + BACK + block_rows]
        scores = jnp.einsum(
            "qrhc,krhc->rhqk",
            query_sub[first_row : first_row + block_rows],
            key_part,
            preferred_element_type=jnp.float32,
        ) * (1.0 / math.sqrt(HD))
        query_index = jnp.arange(block_rows, dtype=jnp.int32)[:, None]
        key_index = jnp.arange(BACK + block_rows, dtype=jnp.int32)[None, :]
        distance = query_index + BACK - key_index
        key_position = anchor + (first_row + key_index - BACK) * dilation + residues
        allowed = (distance >= 0) & (distance <= BACK) & (key_position >= 0)
        scores = jnp.where(allowed, scores, -jnp.inf)
        row_max = jnp.max(scores, axis=-1)
        weights = jnp.exp(scores - row_max[..., None])
        row_sum = jnp.sum(weights, axis=-1)
        weighted = jnp.einsum(
            "rhqk,krhc->qrhc",
            weights.astype(jnp.bfloat16),
            value_part,
            preferred_element_type=jnp.float32,
        )
        sum_rows = row_sum.transpose(2, 0, 1)
        results.append((weighted / sum_rows[..., None]).astype(jnp.bfloat16))
        maxima.append(row_max.transpose(2, 0, 1))
        sums.append(sum_rows)
    result = jnp.concatenate(results, axis=0).reshape(tok_rows, head_count, HD)
    row_max = jnp.concatenate(maxima, axis=0).reshape(tok_rows, head_count)
    row_sum = jnp.concatenate(sums, axis=0).reshape(tok_rows, head_count)
    return (result, row_max, row_sum)


def per_device(query_rows, key_rows, value_rows, out_weight):
    tok_rows = query_rows.shape[0]
    head_count = query_rows.shape[1] // HD
    anchor = lax.axis_index("sp") * tok_rows
    positions = anchor + jnp.arange(tok_rows, dtype=jnp.int32)
    turned_q = rotate(query_rows, positions, head_count, HD)
    turned_k = rotate(key_rows, positions, head_count, HD)
    paired = jnp.stack((turned_k, value_rows))
    pieces = -(-(16 * BACK) // tok_rows)
    held = paired
    gathered = 1
    while gathered < pieces + 1:
        needed = min(gathered, pieces + 1 - gathered)
        arrived = shifted(held[:, held.shape[1] - needed * tok_rows :], "sp", gathered)
        held = jnp.concatenate([arrived, held], axis=1)
        gathered = gathered + needed
    prior = held[:, : held.shape[1] - tok_rows]
    results, maxima, sums = ([], [], [])
    for dilation in DILATIONS:
        reach = BACK * dilation
        key_ext = jnp.concatenate([prior[0, prior.shape[1] - reach :], turned_k], axis=0)
        value_ext = jnp.concatenate([prior[1, prior.shape[1] - reach :], value_rows], axis=0)
        result, row_max, row_sum = pattern_part(
            turned_q, key_ext, value_ext, dilation, anchor, head_count
        )
        results.append(result)
        maxima.append(row_max)
        sums.append(row_sum)
    top = jnp.maximum(jnp.maximum(maxima[0], maxima[1]), maxima[2])
    scales = [sums[i] * jnp.exp(maxima[i] - top) for i in range(3)]
    weighted = scales[0][..., None] * results[0].astype(jnp.float32)
    weighted = weighted + scales[1][..., None] * results[1].astype(jnp.float32)
    weighted = weighted + scales[2][..., None] * results[2].astype(jnp.float32)
    denominator = scales[0] + scales[1] + scales[2]
    mixed = (
        (weighted / denominator[..., None]).reshape(tok_rows, head_count * HD).astype(jnp.bfloat16)
    )
    token_rows = lax.all_to_all(mixed, "tp", split_axis=0, concat_axis=1, tiled=True)
    projected = jnp.dot(
        token_rows,
        lax.all_gather(out_weight, "tp", axis=0, tiled=True),
        preferred_element_type=jnp.float32,
    )
    return projected.astype(jnp.bfloat16)


def solution(mesh):
    return jax.shard_map(
        per_device,
        mesh=mesh,
        in_specs=(P("sp", "tp"), P("sp", "tp"), P("sp", "tp"), P("tp", None)),
        out_specs=P(("sp", "tp"), None),
        check_vma=False,
    )
```

profile of v0, /device:TPU:259, one launch (start us, length us, event | category | flops | bytes accessed | tf_op | source)
XLA Modules:
  0.0 195.9 jit_solution(11508287023331739371)
XLA Ops:
  6.6 1.1 copy.139
  7.7 1.1 copy.140
  8.8 0.2 multiply_cosine_fusion
  9.0 0.2 multiply_subtract_fusion.1
  9.2 0.1 copy.141
  9.4 0.8 pad_maximum_fusion.4
  10.2 3.1 %collective-permute-start = (bf16[2,256,512]{2,1,0:T(8,128)(2,1)}, bf16[2,256,512]{2,1,0:T(8,128)(2,1)S(1)}, u32[]{:S(2)}, u32[]{:S(2)}) collective-permute-start(bf16[2,256,512]{2,1,0:T(8,128)(2,1)} %pad_maximum_fusion.4), channel_id=1, source_target_pairs={{0,2},{2,4},{4,6},{6,8},{8,10},{10,12},{12,14},{14,16},{16,18},{18... | collective-permute-start | bytes 1572872 | tf_op jit(solution)/shard_map/ppermute | solution.py:16
  13.3 4.8 %collective-permute-start.2 = (bf16[2,256,512]{2,1,0:T(8,128)(2,1)}, bf16[2,256,512]{2,1,0:T(8,128)(2,1)}, u32[]{:S(2)}, u32[]{:S(2)}) collective-permute-start(bf16[2,256,512]{2,1,0:T(8,128)(2,1)} %pad_maximum_fusion.4), channel_id=1, source_target_pairs={{0,16},{2,18},{4,20},{6,22},{8,24},{10,26},{12,28},{14,30},{16,32}... | collective-permute-start | bytes 1572872 | tf_op jit(solution)/shard_map/ppermute | solution.py:16
  18.2 0.8 copy.155
  19.1 0.1 copy.144
  19.2 0.3 copy.143
  19.6 0.7 fusion.73
  20.3 4.9 %collective-permute-done = bf16[2,256,512]{2,1,0:T(8,128)(2,1)S(1)} collective-permute-done((bf16[2,256,512]{2,1,0:T(8,128)(2,1)}, bf16[2,256,512]{2,1,0:T(8,128)(2,1)S(1)}, u32[]{:S(2)}, u32[]{:S(2)}) %collective-permute-start) | collective-permute-done | bytes 524320 | tf_op jit(solution)/shard_map/ppermute | solution.py:16
  25.3 3.8 %collective-permute-start.1 = (bf16[2,512,512]{2,1,0:T(8,128)(2,1)S(1)}, bf16[2,512,512]{2,1,0:T(8,128)(2,1)S(1)}, u32[]{:S(2)}, u32[]{:S(2)}) collective-permute-start(bf16[2,512,512]{2,1,0:T(8,128)(2,1)S(1)} %maximum_maximum_fusion.1), channel_id=1, source_target_pairs={{0,4},{2,6},{4,8},{6,10},{8,12},{10,14},{12,16},{14,18},{16,20},{1... | collective-permute-start | bytes 3145736 | tf_op jit(solution)/shard_map/ppermute | solution.py:16
  29.0 0.4 fusion.86
  29.5 0.4 fusion.48
  30.1 36.6 %collective-permute-done.1 = bf16[2,512,512]{2,1,0:T(8,128)(2,1)S(1)} collective-permute-done((bf16[2,512,512]{2,1,0:T(8,128)(2,1)S(1)}, bf16[2,512,512]{2,1,0:T(8,128)(2,1)S(1)}, u32[]{:S(2)}, u32[]{:S(2)}) %collective-permute-start.1) | collective-permute-done | bytes 1048608 | tf_op jit(solution)/shard_map/ppermute | solution.py:16
  66.6 1.5 maximum_maximum_fusion
  68.1 1.9 collective-permute-start.3
  70.1 1.0 fusion.34
  71.1 0.7 slice_bitcast_fusion.4
  71.8 0.8 copy.142
  72.6 0.9 pad_maximum_fusion.5
  73.5 0.8 copy.154
  74.4 1.0 pad_maximum_fusion.6
  75.4 1.2 fusion.87
  76.6 0.4 fusion.46
  77.0 0.6 copy-done.15
  77.6 0.4 fusion.32
  78.0 1.1 reshape.571
  79.1 1.1 constant_dynamic-update-slice_fusion.5
  80.1 39.1 %collective-permute-done.3 = bf16[2,1024,512]{2,1,0:T(8,128)(2,1)} collective-permute-done((bf16[2,1024,512]{2,1,0:T(8,128)(2,1)}, bf16[2,1024,512]{2,1,0:T(8,128)(2,1)}, u32[]{:S(2)}, u32[]{:S(2)}) %collective-permute-start.3) | collective-permute-done | bytes 2097184 | tf_op jit(solution)/shard_map/ppermute | solution.py:16
  119.3 1.7 constant_dynamic-update-slice_fusion.4
  121.0 0.1 constant_dynamic-update-slice_fusion.3
  121.3 2.0 copy-done.1
  123.3 1.7 reshape.557
  125.0 3.9 %fusion.4 = (f32[4,8,64]{2,1,0:T(8,128)S(1)}, f32[4,8,64,192]{3,2,1,0:T(8,128)}) fusion(pred[4,64,192]{2,1,0:T(8,128)(4,1)S(1)} %broadcast_and_fusion.1, bf16[192,4,8,64]{3,2,1,0:T(8,128)(2,1)} %reshape.557, bf16[64,4,8,64]{3,2,1,0:T(8,128)(2,1)S(1)} %bitcast.131), kind=kOutput, calls=%fused_computation.14 | convolution fusion | flops 51509248 | bytes 2678784 | tf_op jit(solution)/shard_map/qrhc,krhc->rhqk/dot_general | solution.py:48
  129.0 1.7 reshape.564
  130.7 2.5 %fusion.7 = f32[4,8,64]{2,1,0:T(8,128)S(1)} fusion(f32[4,8,64,192]{3,2,1,0:T(8,128)} %get-tuple-element.30, f32[4,8,64]{2,1,0:T(8,128)S(1)} %get-tuple-element.29, pred[4,64,192]{2,1,0:T(8,128)(4,1)S(1)} %broadcast_and_fusion.1), kind=kLoop, calls=%fused_computation.17 | loop fusion | flops 1570816 | bytes 1638400 | tf_op jit(solution)/shard_map/reduce_sum | solution.py:62
  133.2 0.8 copy.156
  134.0 3.6 %fusion.28 = f32[64,4,8,64]{0,3,2,1:T(8,128)} fusion(bf16[192,4,8,64]{3,2,1,0:T(8,128)(2,1)} %reshape.564, f32[4,8,64,192]{3,2,1,0:T(8,128)S(1)} %copy-done.4, f32[4,8,64]{2,1,0:T(8,128)S(1)} %get-tuple-element.29, pred[4,64,192]{2,1,0:T(8,128)(4,1)S(1)} %broadcast_and_fusion.1, f32[64,4,8]{0,2,1:T(8,128)S(1)} %bitcast.146), kind=kOutput, calls=%fused_computation.32 | convolution fusion | flops 52297728 | bytes 2949120 | tf_op jit(solution)/shard_map/rhqk,krhc->qrhc/dot_general | solution.py:63
  137.6 2.1 %copy.160 = f32[64,4,8,64]{3,2,1,0:T(8,128)S(1)} copy(f32[64,4,8,64]{0,3,2,1:T(8,128)} %fusion.28) | data formatting | bytes 1048576 | tf_op jit(solution)/shard_map/convert_element_type | solution.py:110
  139.7 0.3 reshape.572
  140.0 1.0 copy.161
  141.0 3.9 %slice_bitcast_fusion = (bf16[2048,512]{1,0:T(8,128)(2,1)}, bf16[2048,512]{1,0:T(8,128)(2,1)S(1)}) fusion(bf16[2,2048,512]{2,1,0:T(8,128)(2,1)} %copy-done.1), kind=kLoop, calls=%fused_computation.7 | loop fusion | bytes 8388608 | tf_op jit(solution)/shard_map/squeeze | solution.py:100
  144.9 0.2 pad_maximum_fusion
  145.0 4.3 %reshape.559 = bf16[144,16,8,64]{3,2,1,0:T(8,128)(2,1)} reshape(bf16[2304,512]{1,0:T(8,128)(2,1)S(1)} %pad_maximum_fusion) | data formatting | bytes 4718592 | tf_op jit(solution)/shard_map/reshape | solution.py:40
  149.3 1.7 pad_maximum_fusion.1
  151.1 4.4 %reshape.566 = bf16[144,16,8,64]{3,2,1,0:T(8,128)(2,1)} reshape(bf16[2304,512]{1,0:T(8,128)(2,1)S(1)} %pad_maximum_fusion.1) | data formatting | bytes 4718592 | tf_op jit(solution)/shard_map/reshape | solution.py:41
  155.5 7.2 %fusion.5 = (f32[16,8,16]{2,1,0:T(8,128)S(1)}, f32[16,8,16,144]{3,2,1,0:T(8,128)S(1)}) fusion(pred[16,16,144]{2,1,0:T(8,128)(4,1)S(1)} %broadcast_and_fusion, bf16[144,16,8,64]{3,2,1,0:T(8,128)(2,1)} %reshape.559, bf16[16,16,8,64]{3,2,1,0:T(8,128)(2,1)S(1)} %bitcast.132), kind=kOutput, calls=%fused_computation.15 | convolution fusion | flops 38631424 | bytes 3846144 | tf_op jit(solution)/shard_map/qrhc,krhc->rhqk/dot_general | solution.py:48
  162.6 0.9 fusion.9
  163.6 6.6 %fusion.53 = f32[16,16,8,64]{3,0,2,1:T(8,128)S(1)} fusion(bf16[144,16,8,64]{3,2,1,0:T(8,128)(2,1)} %reshape.566, f32[16,8,16,144]{3,2,1,0:T(8,128)S(1)} %get-tuple-element.32, f32[16,8,16]{2,1,0:T(8,128)S(1)} %get-tuple-element.31, pred[16,16,144]{2,1,0:T(8,128)(4,1)S(1)} %broadcast_and_fusion, f32[16,16,8]{0,2,1:T(8,128)S(1)} %bitcast.141), kind=kOutput, calls=%fused_computation.55 | convolution fusion | flops 39321600 | bytes 4116480 | tf_op jit(solution)/shard_map/rhqk,krhc->qrhc/dot_general | solution.py:63
  170.3 0.3 copy.164
  170.7 0.3 reshape.573
  170.9 0.2 copy.165
  171.8 0.3 div.64
  172.1 0.3 mul.218
  172.4 0.8 mul.221
  173.3 1.3 mul.222
  174.6 0.8 mul.225
  175.4 2.1 %mul.226 = f32[2,128,512]{1,0,2:T(2,128)} reshape(f32[256,8,64]{0,2,1:T(8,128)} %mul.225) | data formatting | bytes 1048576 | tf_op jit(solution)/shard_map/mul | solution.py:111
  177.5 1.8 fusion.64
  179.3 6.0 %all_to_all.16 = bf16[2,128,512]{1,2,0:T(8,128)(2,1)S(1)} all-to-all(bf16[2,128,512]{1,2,0:T(8,128)(2,1)S(1)} %copy.166), channel_id=1, replica_groups=mesh['sp'=256,'tp'=2] {'tp'}, dimensions={0} | all-to-all | bytes 524288 | tf_op jit(solution)/shard_map/all_to_all | solution.py:116
  185.3 3.7 %convolution_convert_fusion = bf16[128,2048]{1,0:T(8,128)(2,1)} fusion(bf16[128,1024]{0,1:T(8,128)(2,1)S(1)} %bitcast.135, bf16[1024,2048]{1,0:T(8,128)(2,1)} %all-gather.2.cloned.1.call-done), kind=kOutput, calls=%fused_computation.4 | convolution fusion | flops 537133056 | bytes 4980736 | tf_op jit(solution)/shard_map/dot_general | solution.py:117
  (67 shorter events, 1.5 us)
Async XLA Ops:
  6.5 178.7 %all-gather.2.cloned.1.call-start = ((), (), s32[]{:S(2)}) async-start(), calls=%async_computation.1 | async-start | bytes 6291456 | tf_op jit(solution)/shard_map/all_gather | solution.py:119
  7.7 1.7 copy-start
  10.2 15.0 %collective-permute-start = (bf16[2,256,512]{2,1,0:T(8,128)(2,1)}, bf16[2,256,512]{2,1,0:T(8,128)(2,1)S(1)}, u32[]{:S(2)}, u32[]{:S(2)}) collective-permute-start(bf16[2,256,512]{2,1,0:T(8,128)(2,1)} %pad_maximum_fusion.4), channel_id=1, source_target_pairs={{0,2},{2,4},{4,6},{6,8},{8,10},{10,12},{12,14},{14,16},{16,18},{18... | collective-permute-start | bytes 1572872 | tf_op jit(solution)/shard_map/ppermute | solution.py:16
  13.3 65.7 %collective-permute-start.2 = (bf16[2,256,512]{2,1,0:T(8,128)(2,1)}, bf16[2,256,512]{2,1,0:T(8,128)(2,1)}, u32[]{:S(2)}, u32[]{:S(2)}) collective-permute-start(bf16[2,256,512]{2,1,0:T(8,128)(2,1)} %pad_maximum_fusion.4), channel_id=1, source_target_pairs={{0,16},{2,18},{4,20},{6,22},{8,24},{10,26},{12,28},{14,30},{16,32}... | collective-permute-start | bytes 1572872 | tf_op jit(solution)/shard_map/ppermute | solution.py:16
  25.3 41.4 %collective-permute-start.1 = (bf16[2,512,512]{2,1,0:T(8,128)(2,1)S(1)}, bf16[2,512,512]{2,1,0:T(8,128)(2,1)S(1)}, u32[]{:S(2)}, u32[]{:S(2)}) collective-permute-start(bf16[2,512,512]{2,1,0:T(8,128)(2,1)S(1)} %maximum_maximum_fusion.1), channel_id=1, source_target_pairs={{0,4},{2,6},{4,8},{6,10},{8,12},{10,14},{12,16},{14,18},{16,20},{1... | collective-permute-start | bytes 3145736 | tf_op jit(solution)/shard_map/ppermute | solution.py:16
  29.5 40.6 %copy-start.9 = (f32[8,128]{1,0:T(8,128)}, f32[8,128]{1,0:T(8,128)S(1)}, u32[]{:S(2)}) copy-start(f32[8,128]{1,0:T(8,128)S(1)} %get-tuple-element.33) | copy-start | bytes 12292
  29.9 40.2 %copy-start.13 = (f32[8,128]{1,0:T(8,128)}, f32[8,128]{1,0:T(8,128)S(1)}, u32[]{:S(2)}) copy-start(f32[8,128]{1,0:T(8,128)S(1)} %fusion.48) | copy-start | bytes 12292
  30.1 40.0 %copy-start.6 = (bf16[256,512]{0,1:T(8,128)(2,1)S(1)}, bf16[256,512]{0,1:T(8,128)(2,1)}, u32[]{:S(2)}) copy-start(bf16[256,512]{0,1:T(8,128)(2,1)} %copy.155) | copy-start | bytes 786436
  68.1 51.2 %collective-permute-start.3 = (bf16[2,1024,512]{2,1,0:T(8,128)(2,1)}, bf16[2,1024,512]{2,1,0:T(8,128)(2,1)}, u32[]{:S(2)}, u32[]{:S(2)}) collective-permute-start(bf16[2,1024,512]{2,1,0:T(8,128)(2,1)} %maximum_maximum_fusion), channel_id=1, source_target_pairs={{0,8},{2,10},{4,12},{6,14},{8,16},{10,18},{12,20},{14,22},{16,24},... | collective-permute-start | bytes 6291464 | tf_op jit(solution)/shard_map/ppermute | solution.py:16
  74.4 3.2 %copy-start.7 = (bf16[256,512]{0,1:T(8,128)(2,1)S(1)}, bf16[256,512]{0,1:T(8,128)(2,1)}, u32[]{:S(2)}) copy-start(bf16[256,512]{0,1:T(8,128)(2,1)} %copy.154) | copy-start | bytes 786436
  75.3 2.6 %copy-start.8 = (bf16[128,1,8,64]{0,3,2,1:T(8,128)(2,1)S(1)}, bf16[128,1,8,64]{0,3,2,1:T(8,128)(2,1)}, u32[]{:S(2)}) copy-start(bf16[128,1,8,64]{0,3,2,1:T(8,128)(2,1)} %fusion.34) | copy-start | bytes 393220
  76.6 1.4 copy-start.11
  77.0 0.6 copy-start.15
  121.2 2.0 %copy-start.1 = (bf16[2,2048,512]{2,1,0:T(8,128)(2,1)}, bf16[2,2048,512]{2,1,0:T(8,128)(2,1)S(1)}, u32[]{:S(2)}) copy-start(bf16[2,2048,512]{2,1,0:T(8,128)(2,1)S(1)} %get-tuple-element.21) | copy-start | bytes 12582916
  130.7 3.3 %copy-start.4 = (f32[4,8,64,192]{3,2,1,0:T(8,128)S(1)}, f32[4,8,64,192]{3,2,1,0:T(8,128)}, u32[]{:S(2)}) copy-start(f32[4,8,64,192]{3,2,1,0:T(8,128)} %get-tuple-element.30) | copy-start | bytes 4718596
  170.3 1.2 copy-start.5
  170.6 1.1 copy-start.10
  170.6 1.1 copy-start.12
  170.6 1.1 copy-start.14
  170.7 1.1 copy-start.16
  172.1 5.4 %copy-start.2 = (f32[2,128,512]{1,0,2:T(2,128)S(1)}, f32[2,128,512]{1,0,2:T(2,128)}, u32[]{:S(2)}) copy-start(f32[2,128,512]{1,0,2:T(2,128)} %reshape.571) | copy-start | bytes 1572868
  172.1 5.4 %copy-start.3 = (f32[2,128,512]{1,0,2:T(2,128)S(1)}, f32[2,128,512]{1,0,2:T(2,128)}, u32[]{:S(2)}) copy-start(f32[2,128,512]{1,0,2:T(2,128)} %copy.161) | copy-start | bytes 1572868
Sparse Core Ops, SparseCore 0:
  18.3 24.7 all-gather.1
where the time goes:
time: 197 us; the launch traced here: 196 us
  waiting for transfers between devices  80.6 us (41%)
  local copies, waits for them, and re-layouts  39.9 us (20%)
  matrix products  28.1 us (14%)
  between operations  14 us (7%)
  other arithmetic  13.7 us (7%)
  starting transfers between devices  13.6 us (7%)
  blocking collectives  5.97 us (3%)
    ppermute x4, waiting for transfers between devices, shifted(): lax.ppermute(value, axis, [(source, source + steps) for source in range(i...  80.6 us
    ppermute x4, starting transfers between devices, shifted(): lax.ppermute(value, axis, [(source, source + steps) for source in range(i...  13.6 us
    dot_general x4, matrix products, pattern_part(): jnp.einsum('qrhc,krhc->rhqk', query_sub[first_row:first_row + block_rows]...  12.7 us
    dot_general x4, matrix products, pattern_part(): jnp.einsum('rhqk,krhc->qrhc', weights.astype(jnp.bfloat16), value_part, p...  11.6 us
    unnamed x38, local copies, waits for them, and re-layouts  6.39 us
    reshape x2, local copies, waits for them, and re-layouts, pattern_part(): value_sub = value_ext.reshape(BACK + length, dilation, head_count, HD)  6.09 us
    reshape x2, local copies, waits for them, and re-layouts, pattern_part(): key_sub = key_ext.reshape(BACK + length, dilation, head_count, HD)  6.02 us
    all_to_all x1, blocking collectives, per_device(): lax.all_to_all(mixed, 'tp', split_axis=0, concat_axis=1, tiled=True)  5.97 us
  transfers between devices with their start and end apart: 5, of which 3 were waited for; matrix products, arithmetic and copies ran while one was open for 37% of the time, Pallas kernels for 0%

commit v1 on v0

--- a/solution.py
+++ b/solution.py
@@ -8,6 +8,12 @@
 BACK = 128
 THETA = 500000.0
 DILATIONS = (1, 4, 16)
+
+
+def stacked_exchange(block, axis, split, join):
+    pieces = jnp.split(block, lax.axis_size(axis), axis=split)
+    received = lax.all_to_all(jnp.stack(pieces), axis, 0, 0)
+    return jnp.concatenate(received, axis=join)
 
 
 def shifted(value, axis, steps):
@@ -113,7 +119,7 @@
     mixed = (
         (weighted / denominator[..., None]).reshape(tok_rows, head_count * HD).astype(jnp.bfloat16)
     )
-    token_rows = lax.all_to_all(mixed, "tp", split_axis=0, concat_axis=1, tiled=True)
+    token_rows = stacked_exchange(mixed, "tp", 0, 1)
     projected = jnp.dot(
         token_rows,
         lax.all_gather(out_weight, "tp", axis=0, tiled=True),

time: 197 us -> 190 us (0.964)
  local copies, waits for them, and re-layouts: 39.9 us -> 36.1 us
    mul x6 -> x0, local copies, waits for them, and re-layouts: 5.37 us -> none  [the longest x2 2.93 us: per_device(): weighted = weighted + scales[2][..., None] * results[2].astype(jnp.float32)]
    squeeze x1 -> x4, local copies, waits for them, and re-layouts: 0.77 us -> 6.11 us  [per_device(): prior[0, prior.shape[1] - reach:]]
    squeeze x3 -> x0, local copies, waits for them, and re-layouts: 4.59 us -> none  [per_device(): prior[1, prior.shape[1] - reach:]]
    dot_general x4, matrix products: 12.7 us -> 10 us  [pattern_part(): jnp.einsum('qrhc,krhc->rhqk', query_sub[first_row:first_row + block_rows]...]
    unnamed x38 -> x52, local copies, waits for them, and re-layouts: 6.39 us -> 8.55 us
  transfers between devices with their start and end apart: 5 -> 5, of which waited for: 3 -> 3; matrix products, arithmetic and copies ran while one was open for 37% -> 33% of each run, Pallas kernels for 0% -> 0%
where the time goes in v1:
time: 190 us
  waiting for transfers between devices  81.4 us (43%)
  local copies, waits for them, and re-layouts  36.1 us (19%)
  matrix products  26.3 us (14%)
  between operations  14 us (7%)
  starting transfers between devices  13.8 us (7%)
  other arithmetic  12.3 us (6%)
  blocking collectives  5.97 us (3%)
    ppermute x4, waiting for transfers between devices, shifted(): lax.ppermute(value, axis, [(source, source + steps) for source in range(i...  81.4 us
    ppermute x4, starting transfers between devices, shifted(): lax.ppermute(value, axis, [(source, source + steps) for source in range(i...  13.8 us
    dot_general x4, matrix products, pattern_part(): jnp.einsum('rhqk,krhc->qrhc', weights.astype(jnp.bfloat16), value_part, p...  12.6 us
    dot_general x4, matrix products, pattern_part(): jnp.einsum('qrhc,krhc->rhqk', query_sub[first_row:first_row + block_rows]...  10 us
    unnamed x52, local copies, waits for them, and re-layouts  8.55 us
    squeeze x4, local copies, waits for them, and re-layouts, per_device(): prior[0, prior.shape[1] - reach:]  6.11 us
    reshape x2, local copies, waits for them, and re-layouts, pattern_part(): value_sub = value_ext.reshape(BACK + length, dilation, head_count, HD)  6.06 us
    all_to_all x1, blocking collectives, stacked_exchange(): received = lax.all_to_all(jnp.stack(pieces), axis, 0, 0)  5.97 us
  transfers between devices with their start and end apart: 5, of which 3 were waited for; matrix products, arithmetic and copies ran while one was open for 33% of the time, Pallas kernels for 0%

profile of v1, /device:TPU:259, one launch (start us, length us, event | category | flops | bytes accessed | tf_op | source)
XLA Modules:
  0.0 189.8 jit_solution(17181516302657742752)
XLA Ops:
  6.6 1.1 copy.135
  7.7 1.1 copy.136
  8.8 0.2 multiply_cosine_fusion
  9.0 0.2 multiply_subtract_fusion.1
  9.2 0.1 copy.137
  9.4 0.8 pad_maximum_fusion.4
  10.2 3.1 %collective-permute-start = (bf16[2,256,512]{2,1,0:T(8,128)(2,1)}, bf16[2,256,512]{2,1,0:T(8,128)(2,1)S(1)}, u32[]{:S(2)}, u32[]{:S(2)}) collective-permute-start(bf16[2,256,512]{2,1,0:T(8,128)(2,1)} %pad_maximum_fusion.4), channel_id=1, source_target_pairs={{0,2},{2,4},{4,6},{6,8},{8,10},{10,12},{12,14},{14,16},{16,18},{18... | collective-permute-start | bytes 1572872 | tf_op jit(solution)/shard_map/ppermute | solution.py:22
  13.3 4.8 %collective-permute-start.2 = (bf16[2,256,512]{2,1,0:T(8,128)(2,1)}, bf16[2,256,512]{2,1,0:T(8,128)(2,1)}, u32[]{:S(2)}, u32[]{:S(2)}) collective-permute-start(bf16[2,256,512]{2,1,0:T(8,128)(2,1)} %pad_maximum_fusion.4), channel_id=1, source_target_pairs={{0,16},{2,18},{4,20},{6,22},{8,24},{10,26},{12,28},{14,30},{16,32}... | collective-permute-start | bytes 1572872 | tf_op jit(solution)/shard_map/ppermute | solution.py:22
  18.2 0.8 copy.151
  19.1 0.1 copy.140
  19.2 0.3 copy.139
  19.6 0.7 fusion.76
  20.3 4.9 %collective-permute-done = bf16[2,256,512]{2,1,0:T(8,128)(2,1)S(1)} collective-permute-done((bf16[2,256,512]{2,1,0:T(8,128)(2,1)}, bf16[2,256,512]{2,1,0:T(8,128)(2,1)S(1)}, u32[]{:S(2)}, u32[]{:S(2)}) %collective-permute-start) | collective-permute-done | bytes 524320 | tf_op jit(solution)/shard_map/ppermute | solution.py:22
  25.3 3.8 %collective-permute-start.1 = (bf16[2,512,512]{2,1,0:T(8,128)(2,1)S(1)}, bf16[2,512,512]{2,1,0:T(8,128)(2,1)S(1)}, u32[]{:S(2)}, u32[]{:S(2)}) collective-permute-start(bf16[2,512,512]{2,1,0:T(8,128)(2,1)S(1)} %maximum_maximum_fusion.1), channel_id=1, source_target_pairs={{0,4},{2,6},{4,8},{6,10},{8,12},{10,14},{12,16},{14,18},{16,20},{1... | collective-permute-start | bytes 3145736 | tf_op jit(solution)/shard_map/ppermute | solution.py:22
  29.0 0.4 fusion.89
  29.5 0.4 fusion.48
  30.1 36.6 %collective-permute-done.1 = bf16[2,512,512]{2,1,0:T(8,128)(2,1)S(1)} collective-permute-done((bf16[2,512,512]{2,1,0:T(8,128)(2,1)S(1)}, bf16[2,512,512]{2,1,0:T(8,128)(2,1)S(1)}, u32[]{:S(2)}, u32[]{:S(2)}) %collective-permute-start.1) | collective-permute-done | bytes 1048608 | tf_op jit(solution)/shard_map/ppermute | solution.py:22
  66.6 1.5 maximum_maximum_fusion
  68.1 2.1 %collective-permute-start.3 = (bf16[2,1024,512]{2,1,0:T(8,128)(2,1)}, bf16[2,1024,512]{2,1,0:T(8,128)(2,1)}, u32[]{:S(2)}, u32[]{:S(2)}) collective-permute-start(bf16[2,1024,512]{2,1,0:T(8,128)(2,1)} %maximum_maximum_fusion), channel_id=1, source_target_pairs={{0,8},{2,10},{4,12},{6,14},{8,16},{10,18},{12,20},{14,22},{16,24},... | collective-permute-start | bytes 6291464 | tf_op jit(solution)/shard_map/ppermute | solution.py:22
  70.3 1.0 fusion.34
  71.4 0.7 slice_bitcast_fusion.7
  72.0 0.8 copy.138
  72.8 0.9 pad_maximum_fusion.5
  73.7 0.8 copy.150
  74.6 1.0 pad_maximum_fusion.6
  75.6 1.2 fusion.90
  76.8 0.4 fusion.46
  77.2 0.4 fusion.32
  77.6 0.7 pad_maximum_fusion.7
  78.3 1.1 constant_dynamic-update-slice_fusion.5
  79.4 39.9 %collective-permute-done.3 = bf16[2,1024,512]{2,1,0:T(8,128)(2,1)} collective-permute-done((bf16[2,1024,512]{2,1,0:T(8,128)(2,1)}, bf16[2,1024,512]{2,1,0:T(8,128)(2,1)}, u32[]{:S(2)}, u32[]{:S(2)}) %collective-permute-start.3) | collective-permute-done | bytes 2097184 | tf_op jit(solution)/shard_map/ppermute | solution.py:22
  119.3 1.7 constant_dynamic-update-slice_fusion.4
  121.0 0.1 constant_dynamic-update-slice_fusion.1
  121.3 1.9 %copy-done.2 = bf16[2,2048,512]{2,1,0:T(8,128)(2,1)} copy-done((bf16[2,2048,512]{2,1,0:T(8,128)(2,1)}, bf16[2,2048,512]{2,1,0:T(8,128)(2,1)S(1)}, u32[]{:S(2)}) %copy-start.2) | copy-done | bytes 4194328
  123.2 0.9 slice_bitcast_fusion.3
  124.1 0.8 reshape.553
  125.0 1.2 fusion.4
  126.2 1.3 copy-done.3
  127.5 0.9 fusion.7
  128.5 0.7 copy.154
  129.1 3.8 %slice_bitcast_fusion.1 = (bf16[2048,512]{1,0:T(8,128)(2,1)S(1)}, bf16[2048,512]{1,0:T(8,128)(2,1)}) fusion(bf16[2,2048,512]{2,1,0:T(8,128)(2,1)} %copy-done.2), kind=kLoop, calls=%fused_computation.8 | loop fusion | bytes 8388608 | tf_op jit(solution)/shard_map/squeeze | solution.py:105
  133.0 0.2 pad_maximum_fusion
  133.1 4.3 %reshape.555 = bf16[144,16,8,64]{3,2,1,0:T(8,128)(2,1)} reshape(bf16[2304,512]{1,0:T(8,128)(2,1)S(1)} %pad_maximum_fusion) | data formatting | bytes 4718592 | tf_op jit(solution)/shard_map/reshape | solution.py:46
  137.4 7.2 %fusion.5 = (f32[16,8,16]{2,1,0:T(8,128)S(1)}, f32[16,8,16,144]{3,2,1,0:T(8,128)S(1)}) fusion(pred[16,16,144]{2,1,0:T(8,128)(4,1)S(1)} %broadcast_and_fusion, bf16[144,16,8,64]{3,2,1,0:T(8,128)(2,1)} %reshape.555, bf16[16,16,8,64]{3,2,1,0:T(8,128)(2,1)S(1)} %bitcast.147), kind=kOutput, calls=%fused_computation.15 | convolution fusion | flops 38631424 | bytes 3846144 | tf_op jit(solution)/shard_map/qrhc,krhc->rhqk/dot_general | solution.py:54
  144.6 1.4 copy-done.1
  146.1 1.0 fusion.9
  147.1 0.7 reshape.561
  147.9 0.7 reshape.556
  148.7 0.7 copy.144
  149.4 1.1 pad_maximum_fusion.3
  150.5 1.7 reshape.560
  152.2 3.6 %fusion.28 = f32[64,4,8,64]{0,3,2,1:T(8,128)} fusion(bf16[192,4,8,64]{3,2,1,0:T(8,128)(2,1)} %reshape.560, f32[4,8,64,192]{3,2,1,0:T(8,128)S(1)} %copy-done.4, f32[4,8,64]{2,1,0:T(8,128)S(1)} %get-tuple-element.33, pred[4,64,192]{2,1,0:T(8,128)(4,1)S(1)} %copy-done.7, f32[64,4,8]{0,2,1:T(8,128)} %bitcast.161), kind=kOutput, calls=%fused_computation.32 | convolution fusion | flops 52297728 | bytes 2949120 | tf_op jit(solution)/shard_map/rhqk,krhc->qrhc/dot_general | solution.py:69
  155.8 2.1 %copy.156 = f32[64,4,8,64]{3,2,1,0:T(8,128)S(1)} copy(f32[64,4,8,64]{0,3,2,1:T(8,128)} %fusion.28) | data formatting | bytes 1048576 | tf_op jit(solution)/shard_map/convert_element_type | solution.py:116
  157.9 0.3 reshape.570
  158.2 0.2 copy.157
  158.4 1.7 pad_maximum_fusion.1
  160.1 4.3 %reshape.562 = bf16[144,16,8,64]{3,2,1,0:T(8,128)(2,1)} reshape(bf16[2304,512]{1,0:T(8,128)(2,1)S(1)} %pad_maximum_fusion.1) | data formatting | bytes 4718592 | tf_op jit(solution)/shard_map/reshape | solution.py:47
  164.5 7.6 %fusion.53 = f32[16,16,8,64]{3,0,2,1:T(8,128)S(1)} fusion(bf16[144,16,8,64]{3,2,1,0:T(8,128)(2,1)} %reshape.562, f32[16,8,16,144]{3,2,1,0:T(8,128)} %copy-done.1, f32[16,8,16]{2,1,0:T(8,128)S(1)} %get-tuple-element.31, pred[16,16,144]{2,1,0:T(8,128)(4,1)S(1)} %broadcast_and_fusion, f32[16,16,8]{0,2,1:T(8,128)S(1)} %bitcast.156), kind=kOutput, calls=%fused_computation.55 | convolution fusion | flops 39321600 | bytes 4116480 | tf_op jit(solution)/shard_map/rhqk,krhc->qrhc/dot_general | solution.py:69
  172.1 0.3 copy.160
  172.5 0.3 reshape.571
  172.7 0.2 copy.161
  173.1 0.2 fusion.67
  173.3 6.0 %all_to_all.5 = bf16[2,128,512]{1,2,0:T(8,128)(2,1)S(1)} all-to-all(bf16[2,128,512]{1,2,0:T(8,128)(2,1)S(1)} %pad_maximum_fusion.8), channel_id=1, replica_groups=mesh['sp'=256,'tp'=2] {'tp'}, dimensions={0} | all-to-all | bytes 524288 | tf_op jit(solution)/shard_map/all_to_all | solution.py:15
  179.3 3.7 %convolution_convert_fusion = bf16[128,2048]{1,0:T(8,128)(2,1)} fusion(bf16[128,1024]{0,1:T(8,128)(2,1)S(1)} %bitcast.150, bf16[1024,2048]{1,0:T(8,128)(2,1)} %all-gather.2.cloned.1.call-done), kind=kOutput, calls=%fused_computation.4 | convolution fusion | flops 537133056 | bytes 4980736 | tf_op jit(solution)/shard_map/dot_general | solution.py:123
  (73 shorter events, 1.1 us)
Async XLA Ops:
  6.5 172.7 %all-gather.2.cloned.1.call-start = ((), (), s32[]{:S(2)}) async-start(), calls=%async_computation.1 | async-start | bytes 6291456 | tf_op jit(solution)/shard_map/all_gather | solution.py:125
  7.7 1.7 copy-start
  10.2 15.0 %collective-permute-start = (bf16[2,256,512]{2,1,0:T(8,128)(2,1)}, bf16[2,256,512]{2,1,0:T(8,128)(2,1)S(1)}, u32[]{:S(2)}, u32[]{:S(2)}) collective-permute-start(bf16[2,256,512]{2,1,0:T(8,128)(2,1)} %pad_maximum_fusion.4), channel_id=1, source_target_pairs={{0,2},{2,4},{4,6},{6,8},{8,10},{10,12},{12,14},{14,16},{16,18},{18... | collective-permute-start | bytes 1572872 | tf_op jit(solution)/shard_map/ppermute | solution.py:22
  13.3 65.0 %collective-permute-start.2 = (bf16[2,256,512]{2,1,0:T(8,128)(2,1)}, bf16[2,256,512]{2,1,0:T(8,128)(2,1)}, u32[]{:S(2)}, u32[]{:S(2)}) collective-permute-start(bf16[2,256,512]{2,1,0:T(8,128)(2,1)} %pad_maximum_fusion.4), channel_id=1, source_target_pairs={{0,16},{2,18},{4,20},{6,22},{8,24},{10,26},{12,28},{14,30},{16,32}... | collective-permute-start | bytes 1572872 | tf_op jit(solution)/shard_map/ppermute | solution.py:22
  25.3 41.4 %collective-permute-start.1 = (bf16[2,512,512]{2,1,0:T(8,128)(2,1)S(1)}, bf16[2,512,512]{2,1,0:T(8,128)(2,1)S(1)}, u32[]{:S(2)}, u32[]{:S(2)}) collective-permute-start(bf16[2,512,512]{2,1,0:T(8,128)(2,1)S(1)} %maximum_maximum_fusion.1), channel_id=1, source_target_pairs={{0,4},{2,6},{4,8},{6,10},{8,12},{10,14},{12,16},{14,18},{16,20},{1... | collective-permute-start | bytes 3145736 | tf_op jit(solution)/shard_map/ppermute | solution.py:22
  29.5 40.8 %copy-start.12 = (f32[8,128]{1,0:T(8,128)}, f32[8,128]{1,0:T(8,128)S(1)}, u32[]{:S(2)}) copy-start(f32[8,128]{1,0:T(8,128)S(1)} %get-tuple-element.35) | copy-start | bytes 12292
  29.9 40.4 %copy-start.20 = (f32[8,128]{1,0:T(8,128)}, f32[8,128]{1,0:T(8,128)S(1)}, u32[]{:S(2)}) copy-start(f32[8,128]{1,0:T(8,128)S(1)} %fusion.48) | copy-start | bytes 12292
  30.1 40.2 %copy-start.8 = (bf16[256,512]{0,1:T(8,128)(2,1)S(1)}, bf16[256,512]{0,1:T(8,128)(2,1)}, u32[]{:S(2)}) copy-start(bf16[256,512]{0,1:T(8,128)(2,1)} %copy.151) | copy-start | bytes 786436
  68.1 51.2 %collective-permute-start.3 = (bf16[2,1024,512]{2,1,0:T(8,128)(2,1)}, bf16[2,1024,512]{2,1,0:T(8,128)(2,1)}, u32[]{:S(2)}, u32[]{:S(2)}) collective-permute-start(bf16[2,1024,512]{2,1,0:T(8,128)(2,1)} %maximum_maximum_fusion), channel_id=1, source_target_pairs={{0,8},{2,10},{4,12},{6,14},{8,16},{10,18},{12,20},{14,22},{16,24},... | collective-permute-start | bytes 6291464 | tf_op jit(solution)/shard_map/ppermute | solution.py:22
  70.3 55.9 %copy-start.6 = (pred[4,64,192]{2,1,0:T(8,128)(4,1)}, pred[4,64,192]{2,1,0:T(8,128)(4,1)S(1)}, u32[]{:S(2)}) copy-start(pred[4,64,192]{2,1,0:T(8,128)(4,1)S(1)} %broadcast_and_fusion.1) | copy-start | bytes 147460
  74.6 2.6 %copy-start.9 = (bf16[256,512]{0,1:T(8,128)(2,1)S(1)}, bf16[256,512]{0,1:T(8,128)(2,1)}, u32[]{:S(2)}) copy-start(bf16[256,512]{0,1:T(8,128)(2,1)} %copy.150) | copy-start | bytes 786436
  75.5 2.0 %copy-start.10 = (bf16[128,1,8,64]{0,3,2,1:T(8,128)(2,1)S(1)}, bf16[128,1,8,64]{0,3,2,1:T(8,128)(2,1)}, u32[]{:S(2)}) copy-start(bf16[128,1,8,64]{0,3,2,1:T(8,128)(2,1)} %fusion.34) | copy-start | bytes 393220
  76.8 2.6 %copy-start.14 = (f32[8,128]{1,0:T(8,128)}, f32[8,128]{1,0:T(8,128)S(1)}, u32[]{:S(2)}) copy-start(f32[8,128]{1,0:T(8,128)S(1)} %get-tuple-element.37) | copy-start | bytes 12292
  77.2 43.9 %copy-start.22 = (f32[8,128]{1,0:T(8,128)}, f32[8,128]{1,0:T(8,128)S(1)}, u32[]{:S(2)}) copy-start(f32[8,128]{1,0:T(8,128)S(1)} %fusion.46) | copy-start | bytes 12292
  121.3 1.9 %copy-start.2 = (bf16[2,2048,512]{2,1,0:T(8,128)(2,1)}, bf16[2,2048,512]{2,1,0:T(8,128)(2,1)S(1)}, u32[]{:S(2)}) copy-start(bf16[2,2048,512]{2,1,0:T(8,128)(2,1)S(1)} %get-tuple-element.22) | copy-start | bytes 12582916
  126.2 1.3 copy-start.3
  128.3 4.6 %copy-start.11 = (f32[4,8,64]{2,1,0:T(8,128)}, f32[4,8,64]{2,1,0:T(8,128)S(1)}, u32[]{:S(2)}) copy-start(f32[4,8,64]{2,1,0:T(8,128)S(1)} %fusion.7) | copy-start | bytes 24580
  144.6 1.4 copy-start.1
  148.6 3.6 %copy-start.4 = (f32[4,8,64,192]{3,2,1,0:T(8,128)S(1)}, f32[4,8,64,192]{3,2,1,0:T(8,128)}, u32[]{:S(2)}) copy-start(f32[4,8,64,192]{3,2,1,0:T(8,128)} %copy-done.3) | copy-start | bytes 4718596
  148.6 3.6 %copy-start.7 = (pred[4,64,192]{2,1,0:T(8,128)(4,1)S(1)}, pred[4,64,192]{2,1,0:T(8,128)(4,1)}, u32[]{:S(2)}) copy-start(pred[4,64,192]{2,1,0:T(8,128)(4,1)} %copy-done.6) | copy-start | bytes 147460
  172.0 0.9 copy-start.13
  172.0 0.9 copy-start.15
  172.0 0.9 copy-start.16
  172.1 0.9 copy-start.17
  172.1 0.9 copy-start.18
  172.1 0.9 copy-start.19
  172.1 0.9 copy-start.21
  172.1 0.9 copy-start.23
  172.1 1.0 copy-start.5
Sparse Core Ops, SparseCore 0:
  18.3 24.7 all-gather.1
